TPU v7x, 32 devices: a whole 2x2x4 slice. The times are simulated.
32 devices in a mesh: sp: 8 (over z, x), tp: 4 (over y, core).
Axes of the slice: x: 2, y: 2, z: 4, core: 2. Of those that a mesh axis runs over, the one named last changes fastest.
Arguments:
- activations: bfloat16 [4096, 1024], P(('sp', 'tp')), may hold values from -8 to 8, as said below
- input_gain: float32 [1024], replicated, may hold values from 0.5 to 1.5
- query_weight: bfloat16 [1024, 1024], P(None, 'tp'), may hold values from -0.1875 to 0.1875
- key_weight: bfloat16 [1024, 1024], P(None, 'tp'), may hold values from -0.375 to 0.375
- value_weight: bfloat16 [1024, 1024], P(None, 'tp'), may hold values from -0.1875 to 0.1875
- stop_offset: float32 [16], P('tp'), may hold values from -16 to 0, as said below
- output_weight: bfloat16 [1024, 1024], P('tp'), may hold values from -0.1875 to 0.1875
- output_gain: float32 [1024], replicated, may hold values from 0.5 to 1.5
Outputs:
- layer_out: bfloat16 [4096, 1024], P(('sp', 'tp'))
Inputs may be any that keep to these rules, and one draw needn't show every extreme that they name: activations are noise of about unit size plus a mean vector of about unit size shared by each aligned block of 512 rows and different between runs; each row as a whole may also be scaled by a factor between 0.25 and 2; the result is clipped to the range. `stop_offset`: each entry equals minus the natural logarithm of 4096, minus 2, plus the natural logarithm of 3, plus a number between 0 and 0.7.
All inputs are finite; a program needn't handle non-finite values.
Results may differ from a plain program's by a relative error of at most 0.015.
Values may be sent and summed in bfloat16 or wider, within the bound.
A program may use at most 128 MiB of HBM per device.

v0:
```python
import jax
import jax.numpy as jnp
from jax import lax
from jax.sharding import PartitionSpec as P

epsilon = 1e-06


def over_all(shard, axis, dim, block):
    whole = lax.all_gather(shard, axis, axis=dim, tiled=True)
    return block(whole, jnp.int32(0))


def taken_in(shard, axis, dim, absorb, state):
    everything = jax.tree.map(lambda a: lax.all_gather(a, axis, axis=dim, tiled=True), shard)
    return absorb(state, everything, jnp.int32(0))


def own_rows_2(contribution, rows, axis):
    whole = contribution(jnp.int32(0), rows * lax.axis_size(axis)).astype(jnp.bfloat16)
    return lax.psum_scatter(whole, axis, scatter_dimension=0, tiled=True).astype(jnp.float32)


def scaled_rows(row_block, row_gain):
    widened = row_block.astype(jnp.float32)
    spread = jnp.mean(widened * widened, axis=-1, keepdims=True)
    return (widened * lax.rsqrt(spread + epsilon) * row_gain).astype(jnp.bfloat16)


def stopping_terms(queries, key_here, offsets, first_query, first_key):
    score_scale = queries.shape[-1] ** (-0.5)
    scores = jnp.einsum("thd,shd->hts", queries, key_here, preferred_element_type=jnp.float32)
    scores = scores * score_scale + offsets[:, None, None]
    query_pos = first_query + lax.iota(jnp.int32, queries.shape[0])
    key_pos = first_key + lax.iota(jnp.int32, key_here.shape[0])
    earlier = key_pos[None, :] < query_pos[:, None]
    log_keep = jnp.where(earlier[None], jax.nn.log_sigmoid(-scores), 0.0)
    return (scores, earlier, log_keep)


def shard_output(scores, earlier, log_keep, value_here):
    key_count = log_keep.shape[-1]
    upper_ones = (
        lax.iota(jnp.int32, key_count)[:, None] > lax.iota(jnp.int32, key_count)[None, :]
    ).astype(jnp.float32)
    within = jnp.dot(
        log_keep.reshape(-1, key_count), upper_ones, precision=lax.Precision.HIGHEST
    ).reshape(log_keep.shape)
    weights = jnp.where(earlier[None], jnp.exp(jax.nn.log_sigmoid(scores) + within), 0.0).astype(
        jnp.bfloat16
    )
    return jnp.einsum("hts,shd->thd", weights, value_here, preferred_element_type=jnp.float32)


def stick_factors(totals):
    prefix_sums = jnp.cumsum(totals, axis=0)
    return jnp.exp(prefix_sums[-1:] - prefix_sums)


def local(
    activations,
    input_gain,
    query_weight,
    key_weight,
    value_weight,
    stop_offset,
    output_weight,
    output_gain,
):
    normed = scaled_rows(activations, input_gain)
    heads_here = stop_offset.shape[0]
    head_dim = query_weight.shape[1] // heads_here

    def project(portion, offset):
        query_part = jnp.dot(portion, query_weight, preferred_element_type=jnp.float32).astype(
            jnp.bfloat16
        )
        key_part = jnp.dot(portion, key_weight, preferred_element_type=jnp.float32).astype(
            jnp.bfloat16
        )
        value_part = jnp.dot(portion, value_weight, preferred_element_type=jnp.float32).astype(
            jnp.bfloat16
        )
        return jnp.stack([query_part, key_part, value_part], axis=0)

    projected = over_all(normed, "tp", 0, project)
    block_len = projected.shape[1]
    queries = projected[0].reshape(block_len, heads_here, head_dim)
    key_rows = projected[1]
    value_rows = projected[2]
    blocks = lax.axis_size("sp")
    own_block = lax.axis_index("sp")
    first_query = own_block * block_len
    empty_totals = jnp.zeros((blocks, heads_here, block_len), jnp.float32)

    def split_shards(portion):
        return portion.reshape(portion.shape[0] // block_len, block_len, heads_here, head_dim)

    def add_blocks(carried, portions, offset):
        key_shards = split_shards(portions[0])
        value_shards = split_shards(portions[1])

        def add_shard(shard_index, current):
            block_index = offset // block_len + shard_index

            def compute_shard(present):
                outputs, totals = present
                scores, earlier, log_keep = stopping_terms(
                    queries,
                    key_shards[shard_index],
                    stop_offset,
                    first_query,
                    block_index * block_len,
                )
                shard_part = shard_output(scores, earlier, log_keep, value_shards[shard_index])
                outputs = lax.dynamic_update_index_in_dim(outputs, shard_part, block_index, 0)
                totals = lax.dynamic_update_index_in_dim(
                    totals, jnp.sum(log_keep, axis=-1), block_index, 0
                )
                return (outputs, totals)

            def skip_shard(present):
                return present

            return lax.cond(block_index <= own_block, compute_shard, skip_shard, current)

        return lax.fori_loop(0, key_shards.shape[0], add_shard, carried)

    empty_outputs = jnp.zeros((blocks, block_len, heads_here, head_dim), jnp.float32)
    outputs, totals = taken_in(
        (key_rows, value_rows), "sp", 0, add_blocks, (empty_outputs, empty_totals)
    )
    factors = stick_factors(totals)
    attended = jnp.einsum("bht,bthd->thd", factors, outputs, precision=lax.Precision.HIGHEST)
    attended = attended.astype(jnp.bfloat16).reshape(block_len, heads_here * head_dim)
    own_rows = activations.shape[0]

    def project_out(offset, row_count):
        selected = lax.dynamic_slice_in_dim(attended, offset, row_count, 0)
        return jnp.dot(selected, output_weight, preferred_element_type=jnp.float32)

    summed = own_rows_2(project_out, own_rows, "tp")
    return scaled_rows(summed, output_gain)


def solution(mesh):
    in_specs = (
        P(("sp", "tp"), None),
        P(),
        P(None, "tp"),
        P(None, "tp"),
        P(None, "tp"),
        P("tp"),
        P("tp", None),
        P(),
    )
    out_specs = P(("sp", "tp"), None)
    return jax.shard_map(local, mesh=mesh, in_specs=in_specs, out_specs=out_specs, check_vma=False)
```

profile of v0, /device:TPU:24, one launch (start us, length us, event | category | flops | bytes accessed | tf_op | source)
XLA Modules:
  0.0 311.3 jit_solution(2017895014803151200)
XLA Ops:
  9.6 17.7 %all-gather.4.cloned.1.call-done = bf16[512,1024]{1,0:T(8,128)(2,1)} async-done(((bf16[128,1024]{1,0:T(8,128)(2,1)}), bf16[512,1024]{1,0:T(8,128)(2,1)}) %all-gather.4.cloned.1.call-update) | async-done | bytes 1048592 | tf_op jit(solution)/shard_map/all_gather | solution.py:10
  27.3 2.6 convolution_convert_fusion.2
  33.0 45.1 %all-gather.8.cloned.1.call-done = bf16[4096,256]{1,0:T(8,128)(2,1)} async-done(((bf16[512,256]{1,0:T(8,128)(2,1)}), bf16[4096,256]{1,0:T(8,128)(2,1)}) %all-gather.8.cloned.1.call-update) | async-done | bytes 2097168 | tf_op jit(solution)/shard_map/all_gather | solution.py:15
  78.1 7.1 %reshape.74 = bf16[8,512,4,64]{3,2,1,0:T(4,128)(2,1)} reshape(bf16[4096,256]{1,0:T(8,128)(2,1)} %all-gather.8.cloned.1.call-done) | data formatting | bytes 4194304 | tf_op jit(solution)/shard_map/reshape | solution.py:97
  85.2 6.9 %copy.16 = bf16[8,512,4,64]{1,3,2,0:T(8,128)(2,1)} copy(bf16[8,512,4,64]{3,2,1,0:T(4,128)(2,1)} %reshape.74) | data formatting | bytes 4194304 | tf_op jit(solution)/shard_map/while | solution.py:127
  92.1 36.4 %all-gather.6.cloned.1.call-done = bf16[4096,256]{1,0:T(8,128)(2,1)} async-done(((bf16[512,256]{1,0:T(8,128)(2,1)}), bf16[4096,256]{1,0:T(8,128)(2,1)}) %all-gather.6.cloned.1.call-update) | async-done | bytes 2097168 | tf_op jit(solution)/shard_map/all_gather | solution.py:15
  128.5 7.1 %reshape.73 = bf16[8,512,4,64]{3,2,1,0:T(4,128)(2,1)} reshape(bf16[4096,256]{1,0:T(8,128)(2,1)} %all-gather.6.cloned.1.call-done) | data formatting | bytes 4194304 | tf_op jit(solution)/shard_map/reshape | solution.py:97
  135.6 5.6 %copy.15 = bf16[8,512,4,64]{1,3,2,0:T(8,128)(2,1)S(1)} copy(bf16[8,512,4,64]{3,2,1,0:T(4,128)(2,1)} %reshape.73) | data formatting | bytes 4194304 | tf_op jit(solution)/shard_map/while | solution.py:127
  143.7 112.9 %while.17 = (s32[]{:T(128)}, f32[8,512,4,64]{1,3,2,0:T(8,128)}, f32[8,4,512]{2,1,0:T(4,128)S(1)}, s32[]{:T(128)}, bf16[8,512,4,64]{1,3,2,0:T(8,128)(2,1)S(1)}, /...) while((s32[]{:T(128)}, f32[8,512,4,64]{1,3,2,0:T(8,128)}, ...), condition=%wide.region_5.6_spmd, body=%wide.region_1.5_spmd.sunk | while | flops 6747061248 | bytes 14714177 | solution.py:127
  143.7 16.1 %conditional.2 = ((f32[8,512,4,64]{1,3,2,0:T(8,128)}, f32[8,4,512]{2,1,0:T(4,128)S(1)})) conditional(s32[]{:T(128)} %convert_element_type.74, (f32[8,512,4,64]{1,3,2,0:T(8,128)}, f32[8,4,512]{2,1,0:T(4,128)S(1)}) %tuple.49, (s32[]{:T(128)}, bf16[8,512,4,64]{1,3,2,0:T(8,128)(2,1)S(1)}, s32[]{:T(128)}, bf16[8,512,4,64]{1,3,2,0:T(8,128)(2,1)}, ...), branch_computations={%region_2.2_spmd, %region_3.4_spmd} | conditional | flops 6747061248 | bytes 14713974 | solution.py:125
  143.9 4.5 %fusion.11 = (f32[4,512]{1,0:T(4,128)S(1)}, f32[4,512,512]{2,1,0:T(8,128)S(1)}) fusion(f32[4]{0:T(128)S(1)} %get-tuple-element.251, pred[512,512]{0,1:T(8,128)(4,1)S(1)} %broadcast_compare_fusion, bf16[512,4,64]{0,2,1:T(8,128)(2,1)S(1)} %get-tuple-element.250, bf16[8,512,4,64]{1,3,2,0:T(8,128)(2,1)} %get-tuple-element.249, s32[]{:T(128)S(6)} %select_n.24), kind=kOutput, calls=%fused_computation.17 | convolution fusion | flops 145750016 | bytes 4988948 | tf_op jit(solution)/shard_map/while/body/eval_jaxpr/cond/branch_1_fun/thd,shd->hts/dot_general | solution.py:32
  148.4 10.1 %fusion.4 = bf16[4,512,512]{1,2,0:T(8,128)(2,1)S(1)} fusion(f32[4,512,512]{2,1,0:T(8,128)S(1)} %get-tuple-element.306, f32[4]{0:T(128)S(1)} %get-tuple-element.251, pred[512,512]{0,1:T(8,128)(4,1)S(1)} %broadcast_compare_fusion), kind=kOutput, calls=%fused_computation.6 | convolution fusion | flops 6466830336 | bytes 6553616 | tf_op jit(solution)/shard_map/while/body/eval_jaxpr/cond/branch_1_fun/dot_general | solution.py:46
  159.8 16.1 %conditional.2 = ((f32[8,512,4,64]{1,3,2,0:T(8,128)}, f32[8,4,512]{2,1,0:T(4,128)S(1)})) conditional(s32[]{:T(128)} %convert_element_type.74, (f32[8,512,4,64]{1,3,2,0:T(8,128)}, f32[8,4,512]{2,1,0:T(4,128)S(1)}) %tuple.49, (s32[]{:T(128)}, bf16[8,512,4,64]{1,3,2,0:T(8,128)(2,1)S(1)}, s32[]{:T(128)}, bf16[8,512,4,64]{1,3,2,0:T(8,128)(2,1)}, ...), branch_computations={%region_2.2_spmd, %region_3.4_spmd} | conditional | flops 6747061248 | bytes 14713974 | solution.py:125
  160.0 4.5 %fusion.11 = (f32[4,512]{1,0:T(4,128)S(1)}, f32[4,512,512]{2,1,0:T(8,128)S(1)}) fusion(f32[4]{0:T(128)S(1)} %get-tuple-element.251, pred[512,512]{0,1:T(8,128)(4,1)S(1)} %broadcast_compare_fusion, bf16[512,4,64]{0,2,1:T(8,128)(2,1)S(1)} %get-tuple-element.250, bf16[8,512,4,64]{1,3,2,0:T(8,128)(2,1)} %get-tuple-element.249, s32[]{:T(128)S(6)} %select_n.24), kind=kOutput, calls=%fused_computation.17 | convolution fusion | flops 145750016 | bytes 4988948 | tf_op jit(solution)/shard_map/while/body/eval_jaxpr/cond/branch_1_fun/thd,shd->hts/dot_general | solution.py:32
  164.6 10.1 %fusion.4 = bf16[4,512,512]{1,2,0:T(8,128)(2,1)S(1)} fusion(f32[4,512,512]{2,1,0:T(8,128)S(1)} %get-tuple-element.306, f32[4]{0:T(128)S(1)} %get-tuple-element.251, pred[512,512]{0,1:T(8,128)(4,1)S(1)} %broadcast_compare_fusion), kind=kOutput, calls=%fused_computation.6 | convolution fusion | flops 6466830336 | bytes 6553616 | tf_op jit(solution)/shard_map/while/body/eval_jaxpr/cond/branch_1_fun/dot_general | solution.py:46
  175.9 16.1 %conditional.2 = ((f32[8,512,4,64]{1,3,2,0:T(8,128)}, f32[8,4,512]{2,1,0:T(4,128)S(1)})) conditional(s32[]{:T(128)} %convert_element_type.74, (f32[8,512,4,64]{1,3,2,0:T(8,128)}, f32[8,4,512]{2,1,0:T(4,128)S(1)}) %tuple.49, (s32[]{:T(128)}, bf16[8,512,4,64]{1,3,2,0:T(8,128)(2,1)S(1)}, s32[]{:T(128)}, bf16[8,512,4,64]{1,3,2,0:T(8,128)(2,1)}, ...), branch_computations={%region_2.2_spmd, %region_3.4_spmd} | conditional | flops 6747061248 | bytes 14713974 | solution.py:125
  176.1 4.5 %fusion.11 = (f32[4,512]{1,0:T(4,128)S(1)}, f32[4,512,512]{2,1,0:T(8,128)S(1)}) fusion(f32[4]{0:T(128)S(1)} %get-tuple-element.251, pred[512,512]{0,1:T(8,128)(4,1)S(1)} %broadcast_compare_fusion, bf16[512,4,64]{0,2,1:T(8,128)(2,1)S(1)} %get-tuple-element.250, bf16[8,512,4,64]{1,3,2,0:T(8,128)(2,1)} %get-tuple-element.249, s32[]{:T(128)S(6)} %select_n.24), kind=kOutput, calls=%fused_computation.17 | convolution fusion | flops 145750016 | bytes 4988948 | tf_op jit(solution)/shard_map/while/body/eval_jaxpr/cond/branch_1_fun/thd,shd->hts/dot_general | solution.py:32
  180.7 10.1 %fusion.4 = bf16[4,512,512]{1,2,0:T(8,128)(2,1)S(1)} fusion(f32[4,512,512]{2,1,0:T(8,128)S(1)} %get-tuple-element.306, f32[4]{0:T(128)S(1)} %get-tuple-element.251, pred[512,512]{0,1:T(8,128)(4,1)S(1)} %broadcast_compare_fusion), kind=kOutput, calls=%fused_computation.6 | convolution fusion | flops 6466830336 | bytes 6553616 | tf_op jit(solution)/shard_map/while/body/eval_jaxpr/cond/branch_1_fun/dot_general | solution.py:46
  192.1 16.1 %conditional.2 = ((f32[8,512,4,64]{1,3,2,0:T(8,128)}, f32[8,4,512]{2,1,0:T(4,128)S(1)})) conditional(s32[]{:T(128)} %convert_element_type.74, (f32[8,512,4,64]{1,3,2,0:T(8,128)}, f32[8,4,512]{2,1,0:T(4,128)S(1)}) %tuple.49, (s32[]{:T(128)}, bf16[8,512,4,64]{1,3,2,0:T(8,128)(2,1)S(1)}, s32[]{:T(128)}, bf16[8,512,4,64]{1,3,2,0:T(8,128)(2,1)}, ...), branch_computations={%region_2.2_spmd, %region_3.4_spmd} | conditional | flops 6747061248 | bytes 14713974 | solution.py:125
  192.3 4.5 %fusion.11 = (f32[4,512]{1,0:T(4,128)S(1)}, f32[4,512,512]{2,1,0:T(8,128)S(1)}) fusion(f32[4]{0:T(128)S(1)} %get-tuple-element.251, pred[512,512]{0,1:T(8,128)(4,1)S(1)} %broadcast_compare_fusion, bf16[512,4,64]{0,2,1:T(8,128)(2,1)S(1)} %get-tuple-element.250, bf16[8,512,4,64]{1,3,2,0:T(8,128)(2,1)} %get-tuple-element.249, s32[]{:T(128)S(6)} %select_n.24), kind=kOutput, calls=%fused_computation.17 | convolution fusion | flops 145750016 | bytes 4988948 | tf_op jit(solution)/shard_map/while/body/eval_jaxpr/cond/branch_1_fun/thd,shd->hts/dot_general | solution.py:32
  196.8 10.1 %fusion.4 = bf16[4,512,512]{1,2,0:T(8,128)(2,1)S(1)} fusion(f32[4,512,512]{2,1,0:T(8,128)S(1)} %get-tuple-element.306, f32[4]{0:T(128)S(1)} %get-tuple-element.251, pred[512,512]{0,1:T(8,128)(4,1)S(1)} %broadcast_compare_fusion), kind=kOutput, calls=%fused_computation.6 | convolution fusion | flops 6466830336 | bytes 6553616 | tf_op jit(solution)/shard_map/while/body/eval_jaxpr/cond/branch_1_fun/dot_general | solution.py:46
  208.2 16.1 %conditional.2 = ((f32[8,512,4,64]{1,3,2,0:T(8,128)}, f32[8,4,512]{2,1,0:T(4,128)S(1)})) conditional(s32[]{:T(128)} %convert_element_type.74, (f32[8,512,4,64]{1,3,2,0:T(8,128)}, f32[8,4,512]{2,1,0:T(4,128)S(1)}) %tuple.49, (s32[]{:T(128)}, bf16[8,512,4,64]{1,3,2,0:T(8,128)(2,1)S(1)}, s32[]{:T(128)}, bf16[8,512,4,64]{1,3,2,0:T(8,128)(2,1)}, ...), branch_computations={%region_2.2_spmd, %region_3.4_spmd} | conditional | flops 6747061248 | bytes 14713974 | solution.py:125
  208.4 4.5 %fusion.11 = (f32[4,512]{1,0:T(4,128)S(1)}, f32[4,512,512]{2,1,0:T(8,128)S(1)}) fusion(f32[4]{0:T(128)S(1)} %get-tuple-element.251, pred[512,512]{0,1:T(8,128)(4,1)S(1)} %broadcast_compare_fusion, bf16[512,4,64]{0,2,1:T(8,128)(2,1)S(1)} %get-tuple-element.250, bf16[8,512,4,64]{1,3,2,0:T(8,128)(2,1)} %get-tuple-element.249, s32[]{:T(128)S(6)} %select_n.24), kind=kOutput, calls=%fused_computation.17 | convolution fusion | flops 145750016 | bytes 4988948 | tf_op jit(solution)/shard_map/while/body/eval_jaxpr/cond/branch_1_fun/thd,shd->hts/dot_general | solution.py:32
  213.0 10.1 %fusion.4 = bf16[4,512,512]{1,2,0:T(8,128)(2,1)S(1)} fusion(f32[4,512,512]{2,1,0:T(8,128)S(1)} %get-tuple-element.306, f32[4]{0:T(128)S(1)} %get-tuple-element.251, pred[512,512]{0,1:T(8,128)(4,1)S(1)} %broadcast_compare_fusion), kind=kOutput, calls=%fused_computation.6 | convolution fusion | flops 6466830336 | bytes 6553616 | tf_op jit(solution)/shard_map/while/body/eval_jaxpr/cond/branch_1_fun/dot_general | solution.py:46
  224.3 16.1 %conditional.2 = ((f32[8,512,4,64]{1,3,2,0:T(8,128)}, f32[8,4,512]{2,1,0:T(4,128)S(1)})) conditional(s32[]{:T(128)} %convert_element_type.74, (f32[8,512,4,64]{1,3,2,0:T(8,128)}, f32[8,4,512]{2,1,0:T(4,128)S(1)}) %tuple.49, (s32[]{:T(128)}, bf16[8,512,4,64]{1,3,2,0:T(8,128)(2,1)S(1)}, s32[]{:T(128)}, bf16[8,512,4,64]{1,3,2,0:T(8,128)(2,1)}, ...), branch_computations={%region_2.2_spmd, %region_3.4_spmd} | conditional | flops 6747061248 | bytes 14713974 | solution.py:125
  224.5 4.5 %fusion.11 = (f32[4,512]{1,0:T(4,128)S(1)}, f32[4,512,512]{2,1,0:T(8,128)S(1)}) fusion(f32[4]{0:T(128)S(1)} %get-tuple-element.251, pred[512,512]{0,1:T(8,128)(4,1)S(1)} %broadcast_compare_fusion, bf16[512,4,64]{0,2,1:T(8,128)(2,1)S(1)} %get-tuple-element.250, bf16[8,512,4,64]{1,3,2,0:T(8,128)(2,1)} %get-tuple-element.249, s32[]{:T(128)S(6)} %select_n.24), kind=kOutput, calls=%fused_computation.17 | convolution fusion | flops 145750016 | bytes 4988948 | tf_op jit(solution)/shard_map/while/body/eval_jaxpr/cond/branch_1_fun/thd,shd->hts/dot_general | solution.py:32
  229.1 10.1 %fusion.4 = bf16[4,512,512]{1,2,0:T(8,128)(2,1)S(1)} fusion(f32[4,512,512]{2,1,0:T(8,128)S(1)} %get-tuple-element.306, f32[4]{0:T(128)S(1)} %get-tuple-element.251, pred[512,512]{0,1:T(8,128)(4,1)S(1)} %broadcast_compare_fusion), kind=kOutput, calls=%fused_computation.6 | convolution fusion | flops 6466830336 | bytes 6553616 | tf_op jit(solution)/shard_map/while/body/eval_jaxpr/cond/branch_1_fun/dot_general | solution.py:46
  240.4 16.1 %conditional.2 = ((f32[8,512,4,64]{1,3,2,0:T(8,128)}, f32[8,4,512]{2,1,0:T(4,128)S(1)})) conditional(s32[]{:T(128)} %convert_element_type.74, (f32[8,512,4,64]{1,3,2,0:T(8,128)}, f32[8,4,512]{2,1,0:T(4,128)S(1)}) %tuple.49, (s32[]{:T(128)}, bf16[8,512,4,64]{1,3,2,0:T(8,128)(2,1)S(1)}, s32[]{:T(128)}, bf16[8,512,4,64]{1,3,2,0:T(8,128)(2,1)}, ...), branch_computations={%region_2.2_spmd, %region_3.4_spmd} | conditional | flops 6747061248 | bytes 14713974 | solution.py:125
  240.7 4.5 %fusion.11 = (f32[4,512]{1,0:T(4,128)S(1)}, f32[4,512,512]{2,1,0:T(8,128)S(1)}) fusion(f32[4]{0:T(128)S(1)} %get-tuple-element.251, pred[512,512]{0,1:T(8,128)(4,1)S(1)} %broadcast_compare_fusion, bf16[512,4,64]{0,2,1:T(8,128)(2,1)S(1)} %get-tuple-element.250, bf16[8,512,4,64]{1,3,2,0:T(8,128)(2,1)} %get-tuple-element.249, s32[]{:T(128)S(6)} %select_n.24), kind=kOutput, calls=%fused_computation.17 | convolution fusion | flops 145750016 | bytes 4988948 | tf_op jit(solution)/shard_map/while/body/eval_jaxpr/cond/branch_1_fun/thd,shd->hts/dot_general | solution.py:32
  245.2 10.1 %fusion.4 = bf16[4,512,512]{1,2,0:T(8,128)(2,1)S(1)} fusion(f32[4,512,512]{2,1,0:T(8,128)S(1)} %get-tuple-element.306, f32[4]{0:T(128)S(1)} %get-tuple-element.251, pred[512,512]{0,1:T(8,128)(4,1)S(1)} %broadcast_compare_fusion), kind=kOutput, calls=%fused_computation.6 | convolution fusion | flops 6466830336 | bytes 6553616 | tf_op jit(solution)/shard_map/while/body/eval_jaxpr/cond/branch_1_fun/dot_general | solution.py:46
  256.6 2.8 multiply_reduce_fusion
  260.9 41.0 %reduce-scatter.2.cloned.1.call-done = bf16[128,1024]{1,0:T(8,128)(2,1)} async-done(((bf16[512,1024]{1,0:T(8,128)(2,1)}), bf16[128,1024]{1,0:T(8,128)(2,1)}) %reduce-scatter.2.cloned.1.call-update) | async-done | bytes 262160 | tf_op jit(solution)/shard_map/reduce_scatter | solution.py:21
  (61 shorter events, 23.6 us)
Async XLA Ops:
  6.5 252.9 %copy-start = (bf16[256,1024]{1,0:T(8,128)(2,1)S(1)}, bf16[256,1024]{1,0:T(8,128)(2,1)}, u32[]{:S(2)}) copy-start(bf16[256,1024]{1,0:T(8,128)(2,1)} %param.18) | copy-start | bytes 1572868
  6.5 26.0 %copy-start.2 = (bf16[1024,256]{1,0:T(8,128)(2,1)S(1)}, bf16[1024,256]{1,0:T(8,128)(2,1)}, u32[]{:S(2)}) copy-start(bf16[1024,256]{1,0:T(8,128)(2,1)} %param.14) | copy-start | bytes 1572868
  6.5 20.7 %all-gather.4.cloned.1.call-start = ((), (), s32[]{:S(2)}) async-start(), calls=%async_computation.1 | async-start | bytes 1310720 | tf_op jit(solution)/shard_map/all_gather | solution.py:10
  9.5 68.6 %all-gather.8.cloned.1.call-start = ((), (), s32[]{:S(2)}) async-start(), calls=%async_computation.3 | async-start | bytes 2359296 | tf_op jit(solution)/shard_map/all_gather | solution.py:15
  27.3 5.2 %copy-start.1 = (bf16[512,1024]{1,0:T(8,128)(2,1)S(1)}, bf16[512,1024]{1,0:T(8,128)(2,1)}, u32[]{:S(2)}) copy-start(bf16[512,1024]{1,0:T(8,128)(2,1)} %all-gather.4.cloned.1.call-done) | copy-start | bytes 3145732
  29.9 98.6 %all-gather.6.cloned.1.call-start = ((), (), s32[]{:S(2)}) async-start(), calls=%async_computation.2 | async-start | bytes 2359296 | tf_op jit(solution)/shard_map/all_gather | solution.py:15
  32.4 269.4 %reduce-scatter.2.cloned.1.call-start = ((), (), s32[]{:S(2)}) async-start(), calls=%async_computation.4 | async-start | bytes 1310720 | tf_op jit(solution)/shard_map/reduce_scatter | solution.py:21
  135.6 8.1 %copy-start.4 = (f32[4]{0:T(128)S(1)}, f32[4]{0:T(128)}, u32[]{:S(2)}) copy-start(f32[4]{0:T(128)} %param.17) | copy-start | bytes 52
  256.6 46.4 %copy-start.3 = (f32[1024]{0:T(1024)S(1)}, f32[1024]{0:T(1024)}, u32[]{:S(2)}) copy-start(f32[1024]{0:T(1024)} %param.19) | copy-start | bytes 12292
Sparse Core Ops, SparseCore 0:
  9.7 17.5 all-gather.3
  30.0 48.0 all-gather.7
  80.3 48.1 all-gather.5
  261.0 40.8 reduce-scatter.1
where the time goes:
time: 314 us; the launch traced here: 311 us
  waiting for transfers between devices  140 us (45%)
  matrix products  118 us (38%)
  local copies, waits for them, and re-layouts  29.2 us (9%)
  between operations  13.2 us (4%)
  other arithmetic  10.2 us (3%)
    all_gather x2, waiting for transfers between devices, taken_in(): lax.all_gather(a, axis, axis=dim, tiled=True)  81.5 us
    dot_general x7, matrix products, shard_output(): jnp.dot(log_keep.reshape(-1, key_count), upper_ones, precision=lax.Precis...  70.4 us
    reduce_scatter x1, waiting for transfers between devices, own_rows_2(): lax.psum_scatter(whole, axis, scatter_dimension=0, tiled=True)  41 us
    dot_general x7, matrix products, stopping_terms(): jnp.einsum('thd,shd->hts', queries, key_here, preferred_element_type=jnp....  31.8 us
    all_gather x1, waiting for transfers between devices, over_all(): whole = lax.all_gather(shard, axis, axis=dim, tiled=True)  17.7 us
    reshape x2, local copies, waits for them, and re-layouts, split_shards(): portion.reshape(portion.shape[0] // block_len, block_len, heads_here, hea...  14.1 us
    while x2, local copies, waits for them, and re-layouts, add_blocks(): return lax.fori_loop(0, key_shards.shape[0], add_shard, carried)  12.5 us
    dot_general x7, matrix products, shard_output(): jnp.einsum('hts,shd->thd', weights, value_here, preferred_element_type=jn...  8.94 us
  transfers between devices with their start and end apart: 4, of which 4 were waited for; matrix products, arithmetic and copies ran while one was open for 5% of the time, Pallas kernels for 0%

commit v1 on v0

v1 whole, which is shorter than its diff:
```python
import functools

import jax
import jax.numpy as jnp
from jax import lax
from jax.experimental import pallas as pl
from jax.experimental.pallas import tpu as pltpu
from jax.sharding import PartitionSpec as P

epsilon = 1e-06
log2e = 1.4426950408889634
MESH = pl.DeviceIdType.MESH
f32 = jnp.float32
bf16 = jnp.bfloat16


def scaled_rows(widened, row_gain):
    spread = jnp.mean(widened * widened, axis=-1, keepdims=True)
    return (widened * lax.rsqrt(spread + epsilon) * row_gain).astype(bf16)


def layer_kernel(
    S,
    T,
    H,
    dh,
    act,
    gain_in,
    wq,
    wk,
    wv,
    off,
    wo,
    gain_out,
    out,
    xg,
    wg,
    kvs,
    qs,
    kv,
    qr,
    qpad,
    tri,
    acc,
    carry,
    obuf,
    orecv,
    att,
    x_send,
    x_recv,
    w_send,
    w_recv,
    kv_send,
    kv_relay,
    kv_recv,
    q_send,
    q_recv,
    o_send,
    o_recv,
):
    G = S // H
    R = act.shape[0]
    B = R * T
    half = B // 2
    rows = wo.shape[0]
    s = lax.axis_index("sp")
    t = lax.axis_index("tp")
    h, g = s // G, s % G
    y, c = t // 2, t % 2
    partner = y * 2 + 1 - c
    Y = T // 2

    def owner(group):
        turn = s % (2 * G) if group is None else None
        return jnp.where(turn < G, turn, 2 * G - 1 - turn)

    gq = owner(None)

    def block_of(k):
        return k * G + (g if k % 2 == 0 else G - 1 - g)

    def remote(src, dst, send, recv, dev):
        return pltpu.make_async_remote_copy(
            src_ref=src, dst_ref=dst, send_sem=send, recv_sem=recv, device_id=dev, device_id_type=MESH
        )

    started = []

    def go(copy):
        copy.start()
        started.append(copy)
        return copy

    def xrow(index):
        return xg.at[pl.ds(pl.multiple_of(index * R, R), R)]

    def wrow(index):
        return wg.at[pl.ds(pl.multiple_of(index * rows, rows), rows)]

    def x_copy(index, slot, dev):
        return remote(xrow(index), xrow(index), x_send.at[slot], x_recv.at[index], (s, dev))

    def w_copy(src, index, slot, dev):
        return remote(src, wrow(index), w_send.at[slot], w_recv.at[index], (s, dev))

    xg[pl.ds(pl.multiple_of(t * R, R), R)] = scaled_rows(act[...].astype(f32), gain_in[...])
    for e in range(1, Y):
        go(x_copy(t, e, ((y + e) % Y) * 2 + c))
    go(x_copy(t, 0, partner))
    wg[pl.ds(pl.multiple_of(t * rows, rows), rows)] = wo[...]
    high = lax.broadcasted_iota(jnp.int32, (B, half), 0)
    low = lax.broadcasted_iota(jnp.int32, (B, half), 1)
    tri[...] = (high > low).astype(f32).astype(bf16)
    for e in range(1, Y):
        came = ((y + e) % Y) * 2 + c
        x_copy(came, 0, partner).wait_recv()
        go(x_copy(came, Y + e - 1, partner))
    for e in range(1, Y):
        go(w_copy(wo, t, e, ((y + e) % Y) * 2 + c))
    x_copy(partner, 0, partner).wait_recv()
    for e in range(1, Y):
        x_copy(((y + e) % Y) * 2 + 1 - c, 0, partner).wait_recv()

    rows_all = xg[...]
    keys = jnp.dot(rows_all, wk[...], preferred_element_type=f32).astype(bf16)
    values = jnp.dot(rows_all, wv[...], preferred_element_type=f32).astype(bf16)
    for i in range(H):
        cols = slice(i * dh, (i + 1) * dh)
        kvs[i] = jnp.concatenate([keys[:, cols], values[:, cols]], axis=1)
    kv_copies = []
    for d in range(1, H):
        hd = (h + d) % H
        go(remote(kvs.at[hd], kv.at[s], kv_send.at[d], kv_recv.at[s], (hd * G + g, t)))
    for e in range(1, G):
        go(remote(kvs.at[h], kv.at[s], kv_relay.at[e - 1], kv_recv.at[s], (h * G + (g + e) % G, t)))
    kv[s] = kvs[h]
    queries = jnp.dot(rows_all, wq[...], preferred_element_type=f32).astype(bf16)
    for i in range(H):
        cols = slice(i * dh, (i + 1) * dh)
        qs[i] = jnp.concatenate([queries[:half, cols], queries[half:, cols]], axis=1)
    for d in range(1, H):
        hd = (h + d) % H
        go(remote(qs.at[hd], qr.at[s // G], q_send.at[d], q_recv.at[s // G], (hd * G + gq, t)))

    own_q = remote(qs.at[h], qr.at[s // G], q_send.at[0], q_recv.at[s // G], (h * G + gq, t))

    @pl.when(gq != g)
    def _():
        own_q.start()

    @pl.when(gq == g)
    def _():
        qr[s // G] = qs[h]

    def kv_wait(j):
        remote(kvs.at[0], kv.at[j], kv_send.at[0], kv_recv.at[j], (s, t)).wait_recv()

    go(w_copy(wo, t, 0, partner))
    for e in range(1, Y):
        came = ((y + e) % Y) * 2 + c
        w_copy(wo, came, 0, partner).wait_recv()
        go(w_copy(wrow(came), came, Y + e - 1, partner))

    for d in range(1, H):
        hd = (h + d) % H
        j = hd * G + g
        kv_wait(j)
        for e in range(1, G):
            go(
                remote(
                    kv.at[j],
                    kv.at[j],
                    kv_relay.at[d * (G - 1) + e - 1],
                    kv_recv.at[j],
                    (h * G + (g + e) % G, t),
                )
            )

    offset = off[h] * log2e
    factor = dh ** (-0.5) * log2e

    def piece(i, block, width, causal):
        key_tile = kv[block, :width]
        z = lax.dot_general(qpad[i], key_tile, (((1,), (1,)), ((), ())), preferred_element_type=f32)
        z = z * factor + offset
        keep = jnp.maximum(jnp.log2(1.0 + jnp.exp2(jnp.minimum(z, 100.0))), z)
        if causal:
            query_pos = i * half + lax.broadcasted_iota(jnp.int32, (half, width), 0)
            earlier = lax.broadcasted_iota(jnp.int32, (half, width), 1) < query_pos
            lost = jnp.where(earlier, keep, 0.0)
        else:
            lost = keep
        lost_b = lost.astype(bf16)
        first = jnp.dot(lost_b, tri[:width], preferred_element_type=f32)
        after = first
        if width > half:
            last = jnp.dot(lost_b[:, half:], tri[:half], preferred_element_type=f32)
            after = jnp.concatenate([first, last], axis=1)
        weight = jnp.exp2(z - keep - after)
        if causal:
            weight = jnp.where(earlier, weight, 0.0)
        part = jnp.dot(weight.astype(bf16), key_tile, preferred_element_type=f32)
        total = first[:, :1] + lost[:, :1]
        if causal:
            acc[i] = part
            carry[i] = jnp.broadcast_to(total, carry.shape[1:])
        else:
            before = carry[i]
            acc[i] += jnp.exp2(-before) * part
            carry[i] = before + total

    for k in range(H):
        b = block_of(k)
        for e in range(1, G):
            kv_wait(k * G + (g + e) % G)

        @pl.when(b != s)
        def _():
            remote(qs.at[0], qr.at[k], q_send.at[0], q_recv.at[k], (s, t)).wait_recv()

        packed = qr[k]
        blank = jnp.zeros((half, dh), bf16)
        qpad[0] = jnp.concatenate([packed[:, :dh], blank], axis=1)
        qpad[1] = jnp.concatenate([packed[:, dh:], blank], axis=1)
        piece(0, b, half, True)
        piece(1, b, B, True)

        def more(step, unused):
            piece(0, b - 1 - step, B, False)
            piece(1, b - 1 - step, B, False)
            return unused

        lax.fori_loop(0, b, more, 0)
        per = max(half // R, 1)
        for r in range(T):
            chunk = acc[r * R // half, pl.ds(r * R % half, R)]
            obuf[k, r] = jnp.concatenate([chunk[: R // 2, dh:], chunk[R // 2 :, dh:]], axis=1).astype(bf16)
        for e in range(1, T):
            r = (t + e) % T
            go(remote(obuf.at[k, r], orecv.at[t * H + h], o_send.at[k * T + e], o_recv.at[t * H + h], (b, r)))
        own_o = remote(obuf.at[k, t], orecv.at[t * H + h], o_send.at[k * T], o_recv.at[t * H + h], (b, t))

        @pl.when(b != s)
        def _():
            own_o.start()

        @pl.when(b == s)
        def _():
            orecv[t * H + h] = obuf[k, t]

    w_copy(wo, partner, 0, partner).wait_recv()
    for e in range(1, Y):
        w_copy(wo, ((y + e) % Y) * 2 + 1 - c, 0, partner).wait_recv()

    for tt in range(T):
        for hh in range(H):

            @pl.when(jnp.logical_or(tt != t, hh * G + gq != s))
            def _():
                e = tt * H + hh
                remote(obuf.at[0, 0], orecv.at[e], o_send.at[0], o_recv.at[e], (s, t)).wait_recv()

    for p in range(T * H // 2):
        one, two = orecv[2 * p], orecv[2 * p + 1]
        cols = slice(2 * p * dh, (2 * p + 2) * dh)
        att[: R // 2, cols] = jnp.concatenate([one[:, :dh], two[:, :dh]], axis=1)
        att[R // 2 :, cols] = jnp.concatenate([one[:, dh:], two[:, dh:]], axis=1)
    projected = jnp.dot(att[...], wg[...], preferred_element_type=f32)
    out[...] = scaled_rows(projected, gain_out[...])

    for copy in started:
        copy.wait_send()

    @pl.when(gq != g)
    def _():
        own_q.wait_send()

    for k in range(H):
        b = block_of(k)

        @pl.when(b != s)
        def _():
            remote(obuf.at[k, t], orecv.at[t * H + h], o_send.at[k * T], o_recv.at[t * H + h], (b, t)).wait_send()


def solution(mesh):
    S, T = mesh.shape["sp"], mesh.shape["tp"]

    def local(act, gain_in, wq, wk, wv, off, wo, gain_out):
        R, D = act.shape
        H = off.shape[0]
        dh = wq.shape[1] // H
        G = S // H
        B = R * T
        half = B // 2
        vmem = pl.BlockSpec(memory_space=pltpu.VMEM)
        smem = pl.BlockSpec(memory_space=pltpu.SMEM)
        dma = pltpu.SemaphoreType.DMA
        lanes = 2 * dh
        return pl.pallas_call(
            functools.partial(layer_kernel, S, T, H, dh),
            out_shape=jax.ShapeDtypeStruct((R, D), bf16),
            in_specs=[vmem, vmem, vmem, vmem, vmem, smem, vmem, vmem],
            out_specs=vmem,
            scratch_shapes=[
                pltpu.VMEM((B, D), bf16),
                pltpu.VMEM((wo.shape[0] * T, D), bf16),
                pltpu.VMEM((H, B, lanes), bf16),
                pltpu.VMEM((H, half, lanes), bf16),
                pltpu.VMEM((S, B, lanes), bf16),
                pltpu.VMEM((H, half, lanes), bf16),
                pltpu.VMEM((2, half, lanes), bf16),
                pltpu.VMEM((B, half), bf16),
                pltpu.VMEM((2, half, lanes), f32),
                pltpu.VMEM((2, half, lanes), f32),
                pltpu.VMEM((H, T, R // 2, lanes), bf16),
                pltpu.VMEM((T * H, R // 2, lanes), bf16),
                pltpu.VMEM((R, T * H * dh), bf16),
                dma((T,)),
                dma((T,)),
                dma((T,)),
                dma((T,)),
                dma((H,)),
                dma((H * (G - 1),)),
                dma((S,)),
                dma((H,)),
                dma((H,)),
                dma((H * T,)),
                dma((T * H,)),
            ],
            compiler_params=pltpu.CompilerParams(has_side_effects=True, vmem_limit_bytes=50 * 2**20),
        )(act, gain_in.reshape(1, D), wq, wk, wv, off, wo, gain_out.reshape(1, D))

    in_specs = (
        P(("sp", "tp"), None),
        P(),
        P(None, "tp"),
        P(None, "tp"),
        P(None, "tp"),
        P("tp"),
        P("tp", None),
        P(),
    )
    out_specs = P(("sp", "tp"), None)
    return jax.shard_map(local, mesh=mesh, in_specs=in_specs, out_specs=out_specs, check_vma=False)
```

time: 314 us -> 76.2 us (0.24)
  waiting for transfers between devices: 140 us -> 0 us
  matrix products: 118 us -> 0 us
  Pallas kernels: 0 us -> 67.9 us
  local copies, waits for them, and re-layouts: 29.2 us -> 7.85 us
  between operations: 13.2 us -> 0.02 us
  other arithmetic: 10.2 us -> 0 us
    dot_general x25 -> x0, matrix products: 118 us -> none  [the longest x7 70.4 us: shard_output(): jnp.dot(log_keep.reshape(-1, key_count), upper_ones, precision=lax.Precis...]
    all_gather x3 -> x0, waiting for transfers between devices: 99.2 us -> none  [the longest x2 81.5 us: taken_in(): lax.all_gather(a, axis, axis=dim, tiled=True)]
    pallas_call x0 -> x1, Pallas kernels: none -> 67.9 us  [local(): pl.pallas_call(functools.partial(layer_kernel, S, T, H, dh), out_shape=ja...]
    reduce_scatter x1 -> x0, waiting for transfers between devices: 41 us -> none  [own_rows_2(): lax.psum_scatter(whole, axis, scatter_dimension=0, tiled=True)]
    reshape x2 -> x0, local copies, waits for them, and re-layouts: 14.1 us -> none  [split_shards(): portion.reshape(portion.shape[0] // block_len, block_len, heads_here, hea...]
    while x2 -> x0, local copies, waits for them, and re-layouts: 12.5 us -> none  [add_blocks(): return lax.fori_loop(0, key_shards.shape[0], add_shard, carried)]
    unnamed x10 -> x17, local copies, waits for them, and re-layouts: 0.02 us -> 7.85 us
    convert_element_type x2 -> x0, other arithmetic: 3.58 us -> none  [scaled_rows(): (widened * lax.rsqrt(spread + epsilon) * row_gain).astype(jnp.bfloat16)]
  transfers between devices with their start and end apart: 4 -> 0, of which waited for: 4 -> 0; matrix products, arithmetic and copies ran while one was open for 5% -> 0% of each run, Pallas kernels for 0% -> 0%
where the time goes in v1:
time: 76.2 us; the launch traced here: 75.8 us
  Pallas kernels  67.9 us (89%)
  local copies, waits for them, and re-layouts  7.85 us (10%)
    pallas_call x1, Pallas kernels, local(): pl.pallas_call(functools.partial(layer_kernel, S, T, H, dh), out_shape=ja...  67.9 us
    unnamed x17, local copies, waits for them, and re-layouts  7.85 us

profile of v1, /device:TPU:24, one launch (start us, length us, event | category | flops | bytes accessed | tf_op | source)
XLA Modules:
  0.0 75.8 jit_solution(378261987220681150)
XLA Ops:
  0.0 0.0 copy-start.7
  0.0 0.7 copy-done.7
  0.7 0.0 copy-start
  0.7 1.0 %copy-done = bf16[1024,256]{1,0:T(8,128)(2,1)S(1)} copy-done((bf16[1024,256]{1,0:T(8,128)(2,1)S(1)}, bf16[1024,256]{1,0:T(8,128)(2,1)}, u32[]{:S(2)}) %copy-start) | copy-done | bytes 524312
  1.7 0.0 copy-start.1
  1.7 1.0 %copy-done.1 = bf16[1024,256]{1,0:T(8,128)(2,1)S(1)} copy-done((bf16[1024,256]{1,0:T(8,128)(2,1)S(1)}, bf16[1024,256]{1,0:T(8,128)(2,1)}, u32[]{:S(2)}) %copy-start.1) | copy-done | bytes 524312
  2.7 0.0 copy-start.2
  2.7 1.0 %copy-done.2 = bf16[1024,256]{1,0:T(8,128)(2,1)S(1)} copy-done((bf16[1024,256]{1,0:T(8,128)(2,1)S(1)}, bf16[1024,256]{1,0:T(8,128)(2,1)}, u32[]{:S(2)}) %copy-start.2) | copy-done | bytes 524312
  3.8 0.0 copy-start.3
  3.8 1.0 %copy-done.3 = bf16[256,1024]{1,0:T(8,128)(2,1)S(1)} copy-done((bf16[256,1024]{1,0:T(8,128)(2,1)S(1)}, bf16[256,1024]{1,0:T(8,128)(2,1)}, u32[]{:S(2)}) %copy-start.3) | copy-done | bytes 524312
  4.8 0.0 copy-start.4
  4.8 0.9 %copy-done.4 = bf16[128,1024]{1,0:T(8,128)(2,1)S(1)} copy-done((bf16[128,1024]{1,0:T(8,128)(2,1)S(1)}, bf16[128,1024]{1,0:T(8,128)(2,1)}, u32[]{:S(2)}) %copy-start.4) | copy-done | bytes 262168
  5.8 0.0 copy-start.5
  5.8 0.7 copy-done.5
  6.5 0.0 copy-start.6
  6.5 0.7 copy-done.6
  7.2 67.9 %shard_map.82 = bf16[128,1024]{1,0:T(8,128)(2,1)S(1)} custom-call(bf16[128,1024]{1,0:T(8,128)(2,1)S(1)} %copy-done.4, f32[1,1024]{1,0:T(1,128)S(1)} %bitcast.2, bf16[1024,256]{1,0:T(8,128)(2,1)S(1)} %copy-done, bf16[1024,256]{1,0:T(8,128)(2,1)S(1)} %copy-done.1, bf16[1024,256]{1,0:T(8,128)(2,1)S(1)} %copy-done.2, f32[4]{0:T(128)S(1)} %copy-done.7, ...), custom_call_target="tpu_custom_call" | custom-call | tf_op jit(solution)/shard_map/pallas_call | solution.py:300
  75.1 0.7 copy.10
Async XLA Ops:
  0.0 0.7 copy-start.7
  0.7 1.0 %copy-start = (bf16[1024,256]{1,0:T(8,128)(2,1)S(1)}, bf16[1024,256]{1,0:T(8,128)(2,1)}, u32[]{:S(2)}) copy-start(bf16[1024,256]{1,0:T(8,128)(2,1)} %wq.1) | copy-start | bytes 1572868
  1.7 1.0 %copy-start.1 = (bf16[1024,256]{1,0:T(8,128)(2,1)S(1)}, bf16[1024,256]{1,0:T(8,128)(2,1)}, u32[]{:S(2)}) copy-start(bf16[1024,256]{1,0:T(8,128)(2,1)} %wk.1) | copy-start | bytes 1572868
  2.7 1.0 %copy-start.2 = (bf16[1024,256]{1,0:T(8,128)(2,1)S(1)}, bf16[1024,256]{1,0:T(8,128)(2,1)}, u32[]{:S(2)}) copy-start(bf16[1024,256]{1,0:T(8,128)(2,1)} %wv.1) | copy-start | bytes 1572868
  3.8 1.0 %copy-start.3 = (bf16[256,1024]{1,0:T(8,128)(2,1)S(1)}, bf16[256,1024]{1,0:T(8,128)(2,1)}, u32[]{:S(2)}) copy-start(bf16[256,1024]{1,0:T(8,128)(2,1)} %wo.1) | copy-start | bytes 1572868
  4.8 0.9 %copy-start.4 = (bf16[128,1024]{1,0:T(8,128)(2,1)S(1)}, bf16[128,1024]{1,0:T(8,128)(2,1)}, u32[]{:S(2)}) copy-start(bf16[128,1024]{1,0:T(8,128)(2,1)} %act.1) | copy-start | bytes 786436
  5.8 0.7 copy-start.5
  6.5 0.7 copy-start.6

commit v2 on v1

--- a/solution.py
+++ b/solution.py
@@ -26,13 +26,16 @@
     dh,
     act,
     gain_in,
+    wq_hbm,
+    wk_hbm,
+    wv_hbm,
+    off,
+    wo_hbm,
+    gain_out,
+    out,
     wq,
     wk,
     wv,
-    off,
-    wo,
-    gain_out,
-    out,
     xg,
     wg,
     kvs,
@@ -57,12 +60,13 @@
     q_recv,
     o_send,
     o_recv,
+    load,
 ):
     G = S // H
     R = act.shape[0]
     B = R * T
     half = B // 2
-    rows = wo.shape[0]
+    rows = wo_hbm.shape[0]
     s = lax.axis_index("sp")
     t = lax.axis_index("tp")
     h, g = s // G, s % G
@@ -103,11 +107,24 @@
     def w_copy(src, index, slot, dev):
         return remote(src, wrow(index), w_send.at[slot], w_recv.at[index], (s, dev))
 
+    barrier = pltpu.get_barrier_semaphore()
+    for d in range(1, S * T):
+        other = (s * T + t + d) % (S * T)
+        pl.semaphore_signal(barrier, inc=1, device_id=(other // T, other % T), device_id_type=MESH)
+    loads = [
+        pltpu.make_async_copy(wk_hbm, wk, load.at[0]),
+        pltpu.make_async_copy(wv_hbm, wv, load.at[1]),
+        pltpu.make_async_copy(wq_hbm, wq, load.at[2]),
+        pltpu.make_async_copy(wo_hbm, wrow(t), load.at[3]),
+    ]
+    for copy in loads:
+        copy.start()
+
     xg[pl.ds(pl.multiple_of(t * R, R), R)] = scaled_rows(act[...].astype(f32), gain_in[...])
+    pl.semaphore_wait(barrier, S * T - 1)
     for e in range(1, Y):
         go(x_copy(t, e, ((y + e) % Y) * 2 + c))
     go(x_copy(t, 0, partner))
-    wg[pl.ds(pl.multiple_of(t * rows, rows), rows)] = wo[...]
     high = lax.broadcasted_iota(jnp.int32, (B, half), 0)
     low = lax.broadcasted_iota(jnp.int32, (B, half), 1)
     tri[...] = (high > low).astype(f32).astype(bf16)
@@ -115,8 +132,10 @@
         came = ((y + e) % Y) * 2 + c
         x_copy(came, 0, partner).wait_recv()
         go(x_copy(came, Y + e - 1, partner))
-    for e in range(1, Y):
-        go(w_copy(wo, t, e, ((y + e) % Y) * 2 + c))
+    for copy in loads:
+        copy.wait()
+    for e in range(1, Y):
+        go(w_copy(wrow(t), t, e, ((y + e) % Y) * 2 + c))
     x_copy(partner, 0, partner).wait_recv()
     for e in range(1, Y):
         x_copy(((y + e) % Y) * 2 + 1 - c, 0, partner).wait_recv()
@@ -127,12 +146,13 @@
     for i in range(H):
         cols = slice(i * dh, (i + 1) * dh)
         kvs[i] = jnp.concatenate([keys[:, cols], values[:, cols]], axis=1)
-    kv_copies = []
     for d in range(1, H):
         hd = (h + d) % H
         go(remote(kvs.at[hd], kv.at[s], kv_send.at[d], kv_recv.at[s], (hd * G + g, t)))
     for e in range(1, G):
-        go(remote(kvs.at[h], kv.at[s], kv_relay.at[e - 1], kv_recv.at[s], (h * G + (g + e) % G, t)))
+        remote(
+            kvs.at[h], kv.at[s], kv_relay.at[h * (G - 1) + e - 1], kv_recv.at[s], (h * G + (g + e) % G, t)
+        ).start()
     kv[s] = kvs[h]
     queries = jnp.dot(rows_all, wq[...], preferred_element_type=f32).astype(bf16)
     for i in range(H):
@@ -155,26 +175,21 @@
     def kv_wait(j):
         remote(kvs.at[0], kv.at[j], kv_send.at[0], kv_recv.at[j], (s, t)).wait_recv()
 
-    go(w_copy(wo, t, 0, partner))
-    for e in range(1, Y):
-        came = ((y + e) % Y) * 2 + c
-        w_copy(wo, came, 0, partner).wait_recv()
-        go(w_copy(wrow(came), came, Y + e - 1, partner))
-
-    for d in range(1, H):
-        hd = (h + d) % H
-        j = hd * G + g
-        kv_wait(j)
-        for e in range(1, G):
-            go(
-                remote(
-                    kv.at[j],
-                    kv.at[j],
-                    kv_relay.at[d * (G - 1) + e - 1],
-                    kv_recv.at[j],
-                    (h * G + (g + e) % G, t),
-                )
+    def relays(k):
+        j = k * G + g
+        return [
+            remote(
+                kv.at[j], kv.at[j], kv_relay.at[k * (G - 1) + e - 1], kv_recv.at[j], (h * G + (g + e) % G, t)
             )
+            for e in range(1, G)
+        ]
+
+    def relay(k):
+        @pl.when(k != h)
+        def _():
+            kv_wait(k * G + g)
+            for copy in relays(k):
+                copy.start()
 
     offset = off[h] * log2e
     factor = dh ** (-0.5) * log2e
@@ -209,8 +224,11 @@
             acc[i] += jnp.exp2(-before) * part
             carry[i] = before + total
 
+    relay(0)
     for k in range(H):
         b = block_of(k)
+        if k + 1 < H:
+            relay(k + 1)
         for e in range(1, G):
             kv_wait(k * G + (g + e) % G)
 
@@ -231,7 +249,12 @@
             return unused
 
         lax.fori_loop(0, b, more, 0)
-        per = max(half // R, 1)
+        if k == H // 2 - 1:
+            go(w_copy(wrow(t), t, 0, partner))
+            for e in range(1, Y):
+                came = ((y + e) % Y) * 2 + c
+                w_copy(wrow(t), came, 0, partner).wait_recv()
+                go(w_copy(wrow(came), came, Y + e - 1, partner))
         for r in range(T):
             chunk = acc[r * R // half, pl.ds(r * R % half, R)]
             obuf[k, r] = jnp.concatenate([chunk[: R // 2, dh:], chunk[R // 2 :, dh:]], axis=1).astype(bf16)
@@ -248,9 +271,9 @@
         def _():
             orecv[t * H + h] = obuf[k, t]
 
-    w_copy(wo, partner, 0, partner).wait_recv()
-    for e in range(1, Y):
-        w_copy(wo, ((y + e) % Y) * 2 + 1 - c, 0, partner).wait_recv()
+    w_copy(wrow(t), partner, 0, partner).wait_recv()
+    for e in range(1, Y):
+        w_copy(wrow(t), ((y + e) % Y) * 2 + 1 - c, 0, partner).wait_recv()
 
     for tt in range(T):
         for hh in range(H):
@@ -270,6 +293,9 @@
 
     for copy in started:
         copy.wait_send()
+    for k in range(H):
+        for copy in relays(k):
+            copy.wait_send()
 
     @pl.when(gq != g)
     def _():
@@ -294,15 +320,19 @@
         B = R * T
         half = B // 2
         vmem = pl.BlockSpec(memory_space=pltpu.VMEM)
+        hbm = pl.BlockSpec(memory_space=pl.ANY)
         smem = pl.BlockSpec(memory_space=pltpu.SMEM)
         dma = pltpu.SemaphoreType.DMA
         lanes = 2 * dh
         return pl.pallas_call(
             functools.partial(layer_kernel, S, T, H, dh),
             out_shape=jax.ShapeDtypeStruct((R, D), bf16),
-            in_specs=[vmem, vmem, vmem, vmem, vmem, smem, vmem, vmem],
+            in_specs=[vmem, vmem, hbm, hbm, hbm, smem, hbm, vmem],
             out_specs=vmem,
             scratch_shapes=[
+                pltpu.VMEM(wq.shape, bf16),
+                pltpu.VMEM(wk.shape, bf16),
+                pltpu.VMEM(wv.shape, bf16),
                 pltpu.VMEM((B, D), bf16),
                 pltpu.VMEM((wo.shape[0] * T, D), bf16),
                 pltpu.VMEM((H, B, lanes), bf16),
@@ -327,8 +357,9 @@
                 dma((H,)),
                 dma((H * T,)),
                 dma((T * H,)),
+                dma((4,)),
             ],
-            compiler_params=pltpu.CompilerParams(has_side_effects=True, vmem_limit_bytes=50 * 2**20),
+            compiler_params=pltpu.CompilerParams(collective_id=0, has_side_effects=True, vmem_limit_bytes=50 * 2**20),
         )(act, gain_in.reshape(1, D), wq, wk, wv, off, wo, gain_out.reshape(1, D))
 
     in_specs = (

time: 76.2 us -> 67.2 us (0.88)
  Pallas kernels: 67.9 us -> 58.4 us
    pallas_call x1, Pallas kernels: 67.9 us -> 58.4 us  [local(): pl.pallas_call(functools.partial(layer_kernel, S, T, H, dh), out_shape=ja...]
where the time goes in v2:
time: 67.2 us; the launch traced here: 66.3 us
  Pallas kernels  58.4 us (87%)
  local copies, waits for them, and re-layouts  7.85 us (12%)
    pallas_call x1, Pallas kernels, local(): pl.pallas_call(functools.partial(layer_kernel, S, T, H, dh), out_shape=ja...  58.4 us
    unnamed x17, local copies, waits for them, and re-layouts  7.85 us

profile of v2, /device:TPU:24, one launch (start us, length us, event | category | flops | bytes accessed | tf_op | source)
XLA Modules:
  0.0 66.3 jit_solution(12119725226337636902)
XLA Ops:
  0.0 0.0 copy-start.7
  0.0 0.7 copy-done.7
  0.7 0.0 copy-start
  0.7 1.0 %copy-done = bf16[1024,256]{1,0:T(8,128)(2,1)S(1)} copy-done((bf16[1024,256]{1,0:T(8,128)(2,1)S(1)}, bf16[1024,256]{1,0:T(8,128)(2,1)}, u32[]{:S(2)}) %copy-start) | copy-done | bytes 524312
  1.7 0.0 copy-start.1
  1.7 1.0 %copy-done.1 = bf16[1024,256]{1,0:T(8,128)(2,1)S(1)} copy-done((bf16[1024,256]{1,0:T(8,128)(2,1)S(1)}, bf16[1024,256]{1,0:T(8,128)(2,1)}, u32[]{:S(2)}) %copy-start.1) | copy-done | bytes 524312
  2.7 0.0 copy-start.2
  2.7 1.0 %copy-done.2 = bf16[1024,256]{1,0:T(8,128)(2,1)S(1)} copy-done((bf16[1024,256]{1,0:T(8,128)(2,1)S(1)}, bf16[1024,256]{1,0:T(8,128)(2,1)}, u32[]{:S(2)}) %copy-start.2) | copy-done | bytes 524312
  3.8 0.0 copy-start.3
  3.8 1.0 %copy-done.3 = bf16[256,1024]{1,0:T(8,128)(2,1)S(1)} copy-done((bf16[256,1024]{1,0:T(8,128)(2,1)S(1)}, bf16[256,1024]{1,0:T(8,128)(2,1)}, u32[]{:S(2)}) %copy-start.3) | copy-done | bytes 524312
  4.8 0.0 copy-start.4
  4.8 0.9 %copy-done.4 = bf16[128,1024]{1,0:T(8,128)(2,1)S(1)} copy-done((bf16[128,1024]{1,0:T(8,128)(2,1)S(1)}, bf16[128,1024]{1,0:T(8,128)(2,1)}, u32[]{:S(2)}) %copy-start.4) | copy-done | bytes 262168
  5.8 0.0 copy-start.5
  5.8 0.7 %copy-done.5 = f32[1024]{0:T(1024)S(1)} copy-done((f32[1024]{0:T(1024)S(1)}, f32[1024]{0:T(1024)}, u32[]{:S(2)}) %copy-start.5) | copy-done | bytes 4120
  6.5 0.0 copy-start.6
  6.5 0.7 %copy-done.6 = f32[1024]{0:T(1024)S(1)} copy-done((f32[1024]{0:T(1024)S(1)}, f32[1024]{0:T(1024)}, u32[]{:S(2)}) %copy-start.6) | copy-done | bytes 4120
  7.2 58.4 %shard_map.82 = bf16[128,1024]{1,0:T(8,128)(2,1)S(1)} custom-call(bf16[128,1024]{1,0:T(8,128)(2,1)S(1)} %copy-done.4, f32[1,1024]{1,0:T(1,128)S(1)} %bitcast.2, bf16[1024,256]{1,0:T(8,128)(2,1)S(1)} %copy-done, bf16[1024,256]{1,0:T(8,128)(2,1)S(1)} %copy-done.1, bf16[1024,256]{1,0:T(8,128)(2,1)S(1)} %copy-done.2, f32[4]{0:T(128)S(1)} %copy-done.7, ...), custom_call_target="tpu_custom_call" | custom-call | tf_op jit(solution)/shard_map/pallas_call | solution.py:327
  65.6 0.7 %copy.10 = bf16[128,1024]{1,0:T(8,128)(2,1)} copy(bf16[128,1024]{1,0:T(8,128)(2,1)S(1)} %shard_map.82) | data formatting | bytes 524288
Async XLA Ops:
  0.0 0.7 copy-start.7
  0.7 1.0 %copy-start = (bf16[1024,256]{1,0:T(8,128)(2,1)S(1)}, bf16[1024,256]{1,0:T(8,128)(2,1)}, u32[]{:S(2)}) copy-start(bf16[1024,256]{1,0:T(8,128)(2,1)} %wq_hbm.1) | copy-start | bytes 1572868
  1.7 1.0 %copy-start.1 = (bf16[1024,256]{1,0:T(8,128)(2,1)S(1)}, bf16[1024,256]{1,0:T(8,128)(2,1)}, u32[]{:S(2)}) copy-start(bf16[1024,256]{1,0:T(8,128)(2,1)} %wk_hbm.1) | copy-start | bytes 1572868
  2.7 1.0 %copy-start.2 = (bf16[1024,256]{1,0:T(8,128)(2,1)S(1)}, bf16[1024,256]{1,0:T(8,128)(2,1)}, u32[]{:S(2)}) copy-start(bf16[1024,256]{1,0:T(8,128)(2,1)} %wv_hbm.1) | copy-start | bytes 1572868
  3.8 1.0 %copy-start.3 = (bf16[256,1024]{1,0:T(8,128)(2,1)S(1)}, bf16[256,1024]{1,0:T(8,128)(2,1)}, u32[]{:S(2)}) copy-start(bf16[256,1024]{1,0:T(8,128)(2,1)} %wo_hbm.1) | copy-start | bytes 1572868
  4.8 0.9 %copy-start.4 = (bf16[128,1024]{1,0:T(8,128)(2,1)S(1)}, bf16[128,1024]{1,0:T(8,128)(2,1)}, u32[]{:S(2)}) copy-start(bf16[128,1024]{1,0:T(8,128)(2,1)} %act.1) | copy-start | bytes 786436
  5.8 0.7 %copy-start.5 = (f32[1024]{0:T(1024)S(1)}, f32[1024]{0:T(1024)}, u32[]{:S(2)}) copy-start(f32[1024]{0:T(1024)} %param.9) | copy-start | bytes 12292
  6.5 0.7 %copy-start.6 = (f32[1024]{0:T(1024)S(1)}, f32[1024]{0:T(1024)}, u32[]{:S(2)}) copy-start(f32[1024]{0:T(1024)} %param.15) | copy-start | bytes 12292
